TPU v7x, 32 devices: a whole 2x2x4 slice. The times are simulated.
32 devices in a mesh: sp: 16 (over z, y, x), tp: 2 (over core).
Axes of the slice: x: 2, y: 2, z: 4, core: 2. Of those that a mesh axis runs over, the one named last changes fastest.
Arguments:
- stream_in: bfloat16 [2048, 2048], P(('sp', 'tp')), may hold values from -6 to 6
- query_compressed: bfloat16 [2048, 512], P('sp'), may hold values from -6 to 6
- keyvalue_compressed: bfloat16 [2048, 256], P('sp'), may hold values from -6 to 6
- rope_key: bfloat16 [2048, 64], P('sp'), may hold values from -153 to 153
- query_norm_gain: float32 [512], replicated, may hold values from 0.1 to 1.9
- keyvalue_norm_gain: float32 [256], replicated, may hold values from 0.1 to 1.9
- query_up_weight: bfloat16 [512, 3072], replicated, may hold values from -0.625 to 0.625
- keyvalue_up_weight: bfloat16 [256, 4096], replicated, may hold values from -0.375 to 0.375
- out_proj: bfloat16 [2048, 2048], replicated, may hold values from -0.5 to 0.5
- ffn_gain: float32 [2048], replicated, may hold values from 0.1 to 1.9
- expert_ids: int32 [2048, 4], P(('sp', 'tp')), may hold values from 0 to 15, all different within a row; in each aligned block of 64 rows (0 to 63, 64 to 127, ...) at most 32 rows name the same one
- expert_weights: float32 [2048, 4], P(('sp', 'tp')), may hold values from 0.1 to 1
- expert_gate: bfloat16 [16, 2048, 512], P('sp', None, 'tp'), may hold values from -0.125 to 0.125
- expert_up: bfloat16 [16, 2048, 512], P('sp', None, 'tp'), may hold values from -0.125 to 0.125
- expert_down: bfloat16 [16, 512, 2048], P('sp', 'tp'), may hold values from -0.25 to 0.25
- shared_gate: bfloat16 [2048, 512], replicated, may hold values from -0.125 to 0.125
- shared_up: bfloat16 [2048, 512], replicated, may hold values from -0.125 to 0.125
- shared_down: bfloat16 [512, 2048], replicated, may hold values from -0.25 to 0.25
Outputs:
- layer_out: bfloat16 [2048, 2048], P(('sp', 'tp'))
Inputs may be any that keep to these rules, and one draw needn't show every extreme that they name: `expert_ids`: each row names 4 different experts. Among the rows of one device (aligned blocks of 64 rows in token order) no expert is named by more than 32 rows, a bound that some block reaches of some device.
All inputs are finite; a program needn't handle non-finite values.
Results may differ from a plain program's by a relative error of at most 0.02.
The roundings to bfloat16 on the way count: a program that leaves them out, or rounds other values in their place, can miss the bound.
Values may be sent and summed in bfloat16 or wider, within the bound.
A program may use at most 128 MiB of HBM per device.

v0:
```python
import jax
import jax.numpy as jnp
from jax import lax
from jax.sharding import PartitionSpec as P

KEY_PLAIN_WIDTH = 128
ROTARY_WIDTH = 64
VALUE_HEAD_WIDTH = 128
epsilon = 1e-06
routed_scale = 2.5
theta_base = 10000.0


def rms_scale(values, scales):
    widened = values.astype(jnp.float32)
    inverse = lax.rsqrt(jnp.mean(widened * widened, axis=-1, keepdims=True) + epsilon)
    return widened * inverse * scales


def turn_tables(positions, rot_width):
    half_width = rot_width // 2
    frequency = theta_base ** (-(jnp.arange(half_width, dtype=jnp.float32) * 2.0) / rot_width)
    angles = positions.astype(jnp.float32)[:, None] * frequency[None, :]
    return (jnp.cos(angles), jnp.sin(angles))


def turn(values, cos_part, sine_part):
    lower_half, upper_half = jnp.split(values, 2, axis=-1)
    return jnp.concatenate(
        [
            lower_half * cos_part - upper_half * sine_part,
            upper_half * cos_part + lower_half * sine_part,
        ],
        axis=-1,
    )


def key_span(piece_rows):
    for candidate in (1024, 512, 256, 128):
        return candidate
    return piece_rows


def expand_keys(lat_block, rot_block, key_pos, keyvalue_norm_gain, keyval_cols, head_count):
    keyval_normed = rms_scale(lat_block, keyvalue_norm_gain).astype(jnp.bfloat16)
    keyvals = jnp.dot(keyval_normed, keyval_cols, preferred_element_type=jnp.float32).astype(
        jnp.bfloat16
    )
    keyvals = keyvals.reshape(lat_block.shape[0], head_count, KEY_PLAIN_WIDTH + VALUE_HEAD_WIDTH)
    cos_part, sine_part = turn_tables(key_pos, rot_block.shape[-1])
    shared_rot = turn(rot_block.astype(jnp.float32), cos_part, sine_part).astype(jnp.bfloat16)
    return (keyvals[:, :, :KEY_PLAIN_WIDTH], keyvals[:, :, KEY_PLAIN_WIDTH:], shared_rot)


def absorb(carried, queries, key_part, value_part, shared_rot):
    run_max, run_sum, run_acc = carried
    scores = jnp.einsum(
        "qhd,khd->qhk",
        queries[:, :, :KEY_PLAIN_WIDTH],
        key_part,
        preferred_element_type=jnp.float32,
    )
    scores = scores + jnp.einsum(
        "qhr,kr->qhk",
        queries[:, :, KEY_PLAIN_WIDTH:],
        shared_rot,
        preferred_element_type=jnp.float32,
    )
    new_max = jnp.maximum(run_max, jnp.max(scores, axis=-1))
    factor = jnp.exp(run_max - new_max)
    weights = jnp.exp(scores - new_max[:, :, None])
    new_sum = run_sum * factor + jnp.sum(weights, axis=-1)
    new_acc = run_acc * factor[:, :, None] + jnp.einsum(
        "qhk,khd->qhd", weights.astype(jnp.bfloat16), value_part, preferred_element_type=jnp.float32
    )
    return (new_max, new_sum, new_acc)


def attend_all(
    queries, lat_shard, rot_shard, keyvalue_norm_gain, keyval_cols, head_count, place_rows
):
    query_rows = queries.shape[0]
    initial = (
        jnp.full((query_rows, head_count), -jnp.inf, jnp.float32),
        jnp.zeros((query_rows, head_count), jnp.float32),
        jnp.zeros((query_rows, head_count, VALUE_HEAD_WIDTH), jnp.float32),
    )
    lat_piece = lax.all_gather(lat_shard, "sp", axis=0, tiled=True)
    rot_piece = lax.all_gather(rot_shard, "sp", axis=0, tiled=True)
    span_rows = key_span(lat_piece.shape[0])
    block_total = lat_piece.shape[0] // span_rows

    def one_block(inner_carried, block_index):
        lat_block = lax.dynamic_slice_in_dim(lat_piece, block_index * span_rows, span_rows, 0)
        rot_block = lax.dynamic_slice_in_dim(rot_piece, block_index * span_rows, span_rows, 0)
        key_pos = place_rows(block_index * span_rows + jnp.arange(span_rows, dtype=jnp.int32))
        key_part, value_part, shared_rot = expand_keys(
            lat_block, rot_block, key_pos, keyvalue_norm_gain, keyval_cols, head_count
        )
        return (absorb(inner_carried, queries, key_part, value_part, shared_rot), None)

    result, _ = lax.scan(one_block, initial, jnp.arange(block_total, dtype=jnp.int32))
    return result


def shards(
    stream_in,
    query_compressed,
    keyvalue_compressed,
    rope_key,
    query_norm_gain,
    keyvalue_norm_gain,
    query_up_weight,
    keyvalue_up_weight,
    out_proj,
    ffn_gain,
    expert_ids,
    expert_weights,
    expert_gate,
    expert_up,
    expert_down,
    shared_gate,
    shared_up,
    shared_down,
):
    full_gate, full_up, full_down = (
        lax.all_gather(expert_gate, "tp", axis=2, tiled=True),
        lax.all_gather(expert_up, "tp", axis=2, tiled=True),
        lax.all_gather(expert_down, "tp", axis=1, tiled=True),
    )
    tok_rows = query_compressed.shape[0]
    head_width = KEY_PLAIN_WIDTH + ROTARY_WIDTH
    pair_width = KEY_PLAIN_WIDTH + VALUE_HEAD_WIDTH
    all_heads = query_up_weight.shape[1] // head_width
    sp_index = lax.axis_index("sp")
    tp_index = lax.axis_index("tp")
    own_pos = sp_index * tok_rows + jnp.arange(tok_rows, dtype=jnp.int32)
    query_normed = rms_scale(query_compressed, query_norm_gain).astype(jnp.bfloat16)
    local_heads = all_heads // 2
    query_cols = lax.dynamic_slice_in_dim(
        query_up_weight, tp_index * local_heads * head_width, local_heads * head_width, 1
    )
    keyval_cols = lax.dynamic_slice_in_dim(
        keyvalue_up_weight, tp_index * local_heads * pair_width, local_heads * pair_width, 1
    )
    raw_query = jnp.dot(
        query_normed, query_cols, preferred_element_type=jnp.float32
    ) * head_width ** (-0.5)
    raw_query = raw_query.reshape(tok_rows, local_heads, head_width)
    cos_part, sine_part = turn_tables(own_pos, ROTARY_WIDTH)
    turned = turn(raw_query[:, :, KEY_PLAIN_WIDTH:], cos_part[:, None, :], sine_part[:, None, :])
    queries = jnp.concatenate([raw_query[:, :, :KEY_PLAIN_WIDTH], turned], axis=-1).astype(
        jnp.bfloat16
    )

    def place_whole(whole_rows):
        return whole_rows

    run_max, run_sum, run_acc = attend_all(
        queries,
        keyvalue_compressed,
        rope_key,
        keyvalue_norm_gain,
        keyval_cols,
        local_heads,
        place_whole,
    )
    local_out = (
        (run_acc / run_sum[:, :, None])
        .astype(jnp.bfloat16)
        .reshape(tok_rows, local_heads * VALUE_HEAD_WIDTH)
    )
    attended = lax.all_to_all(local_out, "tp", split_axis=0, concat_axis=1, tiled=True)
    projected = jnp.dot(attended, out_proj, preferred_element_type=jnp.float32)
    stream = (stream_in.astype(jnp.float32) + projected).astype(jnp.bfloat16)
    normed = rms_scale(stream, ffn_gain).astype(jnp.bfloat16)
    shares = (
        routed_scale * expert_weights / jnp.sum(expert_weights, axis=-1, keepdims=True)
    ).astype(jnp.bfloat16)
    moe_rows = stream_in.shape[0]
    top_count = expert_ids.shape[1]
    sp_count = lax.axis_size("sp")
    local_experts = expert_gate.shape[0]
    expert_count = local_experts * sp_count
    capacity = 2 * moe_rows * top_count // expert_count
    flat_ids = expert_ids.reshape(-1)
    hot_ids = (flat_ids[:, None] == jnp.arange(expert_count, dtype=jnp.int32)[None, :]).astype(
        jnp.int32
    )
    rank_ids = jnp.sum((jnp.cumsum(hot_ids, axis=0) - hot_ids) * hot_ids, axis=1)
    slot_ids = flat_ids * capacity + rank_ids
    hot_slots = (
        slot_ids[:, None] == jnp.arange(expert_count * capacity, dtype=jnp.int32)[None, :]
    ).reshape(moe_rows, top_count, expert_count * capacity)
    sender_map = jnp.any(hot_slots, axis=1).astype(jnp.bfloat16)
    combine = jnp.sum(jnp.where(hot_slots, shares[:, :, None], jnp.zeros((), jnp.bfloat16)), axis=1)
    outgoing = jnp.einsum(
        "ts,td->sd", sender_map, normed, preferred_element_type=jnp.float32
    ).astype(jnp.bfloat16)
    outgoing = outgoing.reshape(sp_count, local_experts, capacity, normed.shape[1])
    arrived = lax.all_to_all(outgoing, "sp", split_axis=0, concat_axis=0, tiled=True)
    gate_act = jnp.einsum("secd,edf->secf", arrived, full_gate, preferred_element_type=jnp.float32)
    up_act = jnp.einsum("secd,edf->secf", arrived, full_up, preferred_element_type=jnp.float32)
    inner_act = (jax.nn.silu(gate_act) * up_act).astype(jnp.bfloat16)
    half_hidden = inner_act.shape[-1] // 2
    first_half = jnp.einsum(
        "secf,efd->secd",
        inner_act[..., :half_hidden],
        full_down[:, :half_hidden],
        preferred_element_type=jnp.float32,
    ).astype(jnp.bfloat16)
    second_half = jnp.einsum(
        "secf,efd->secd",
        inner_act[..., half_hidden:],
        full_down[:, half_hidden:],
        preferred_element_type=jnp.float32,
    ).astype(jnp.bfloat16)
    summed = (first_half.astype(jnp.float32) + second_half.astype(jnp.float32)).astype(jnp.bfloat16)
    returned = lax.all_to_all(summed, "sp", split_axis=0, concat_axis=0, tiled=True)
    routed = jnp.dot(
        combine,
        returned.reshape(expert_count * capacity, normed.shape[1]),
        preferred_element_type=jnp.float32,
    )
    shared_inner = (
        jax.nn.silu(jnp.dot(normed, shared_gate, preferred_element_type=jnp.float32))
        * jnp.dot(normed, shared_up, preferred_element_type=jnp.float32)
    ).astype(jnp.bfloat16)
    shared_out = jnp.dot(shared_inner, shared_down, preferred_element_type=jnp.float32)
    return (stream.astype(jnp.float32) + routed + shared_out).astype(jnp.bfloat16)


def solution(mesh):
    in_specs = (
        P(("sp", "tp"), None),
        P("sp", None),
        P("sp", None),
        P("sp", None),
        P(),
        P(),
        P(),
        P(),
        P(),
        P(),
        P(("sp", "tp"), None),
        P(("sp", "tp"), None),
        P("sp", None, "tp"),
        P("sp", None, "tp"),
        P("sp", "tp", None),
        P(),
        P(),
        P(),
    )
    out_specs = P(("sp", "tp"), None)
    return jax.shard_map(shards, mesh=mesh, in_specs=in_specs, out_specs=out_specs, check_vma=False)
```

profile of v0, /device:TPU:12, one launch (start us, length us, event | category | flops | bytes accessed | tf_op | source)
XLA Modules:
  0.0 256.1 jit_solution(11174466686180340704)
XLA Ops:
  10.1 2.2 convolution_multiply_fusion
  14.3 35.2 %all_gather.16 = bf16[2048,64]{0,1:T(8,128)(2,1)} all-gather(bf16[128,64]{0,1:T(8,128)(2,1)S(1)} %copy-done.13), channel_id=1, replica_groups=mesh['sp'=16,'tp'=2] {'sp'}, dimensions={0}, use_global_device_ids=true | all-gather | bytes 278528 | tf_op jit(solution)/shard_map/all_gather | solution.py:89
  51.3 2.3 constant_dynamic-slice_fusion
  53.6 12.2 %all-gather.5.cloned.1.call-done = bf16[2048,256]{1,0:T(8,128)(2,1)} async-done(((bf16[128,256]{1,0:T(8,128)(2,1)}), bf16[2048,256]{1,0:T(8,128)(2,1)}) %all-gather.5.cloned.1.call-update) | async-done | bytes 1048592 | tf_op jit(solution)/shard_map/all_gather | solution.py:88
  65.8 45.4 %while.15 = (s32[]{:T(128)}, f32[128,8]{0,1:T(8,128)S(1)}, f32[128,8]{0,1:T(8,128)S(1)}, f32[128,8,128]{0,2,1:T(8,128)}, s32[2]{0:T(128)S(1)}, /*index=5*/bf16[2...) while((s32[]{:T(128)}, f32[128,8]{0,1:T(8,128)S(1)}, ...), condition=%wide.region_5.6_spmd.clone, body=%wide.region_1.5_spmd.clone.sunk | while | flops 1756078208 | bytes 72443560 | solution.py:102
  68.4 2.7 %convolution_convert_fusion.5 = bf16[1024,2048]{1,0:T(8,128)(2,1)S(1)} fusion(bf16[256,2048]{1,0:T(8,128)(2,1)} %get-tuple-element.279, f32[256]{0:T(256)S(1)} %get-tuple-element.278, f32[1024]{0:T(1024)S(1)} %add_rsqrt_fusion.4, bf16[2048,256]{1,0:T(8,128)(2,1)} %get-tuple-element.277, s32[]{:T(128)S(6)} %select_n.22), kind=kOutput, calls=%fused_computation.2.clone.1 | convolution fusion | flops 1076887552 | bytes 5772292 | tf_op jit(solution)/shard_map/while/body/eval_jaxpr/dot_general | solution.py:46
  72.8 2.7 %fusion.132 = f32[8,1024,128]{2,1,0:T(8,128)} fusion(bf16[1024,8,128]{2,1,0:T(8,128)(2,1)S(1)} %get-tuple-element.238, bf16[128,8,192]{2,0,1:T(8,128)(2,1)S(1)} %get-tuple-element.280), kind=kOutput, calls=%fused_computation.7.clone.1 | convolution fusion | flops 268435456 | bytes 6553600 | tf_op jit(solution)/shard_map/while/body/eval_jaxpr/qhd,khd->qhk/dot_general | solution.py:57
  77.9 5.0 %fusion.133 = (f32[128,8]{0,1:T(8,128)S(1)}, f32[128,8,1024]{0,2,1:T(8,128)}) fusion(bf16[128,8,192]{0,2,1:T(8,128)(2,1)S(1)} %copy.109, bf16[1024,32]{0,1:T(8,128)(2,1)} %get-tuple-element.236, bf16[1024,32]{0,1:T(8,128)(2,1)} %get-tuple-element.237, f32[8,1024,128]{2,1,0:T(8,128)} %fusion.132), kind=kOutput, calls=%fused_computation.121.clone.1 | convolution fusion | flops 136576000 | bytes 8654848 | tf_op jit(solution)/shard_map/while/body/eval_jaxpr/qhr,kr->qhk/dot_general | solution.py:63
  83.0 2.9 %fusion.134 = f32[128,8]{0,1:T(8,128)S(1)} fusion(f32[128,8,1024]{0,2,1:T(8,128)} %get-tuple-element.240, f32[128,8]{0,1:T(8,128)S(1)} %select_maximum_fusion.2), kind=kLoop, calls=%fused_computation.4.clone.1 | loop fusion | flops 2096128 | bytes 4202496 | tf_op jit(solution)/shard_map/while/body/eval_jaxpr/reduce_sum | solution.py:72
  91.1 2.7 %convolution_convert_fusion.5 = bf16[1024,2048]{1,0:T(8,128)(2,1)S(1)} fusion(bf16[256,2048]{1,0:T(8,128)(2,1)} %get-tuple-element.279, f32[256]{0:T(256)S(1)} %get-tuple-element.278, f32[1024]{0:T(1024)S(1)} %add_rsqrt_fusion.4, bf16[2048,256]{1,0:T(8,128)(2,1)} %get-tuple-element.277, s32[]{:T(128)S(6)} %select_n.22), kind=kOutput, calls=%fused_computation.2.clone.1 | convolution fusion | flops 1076887552 | bytes 5772292 | tf_op jit(solution)/shard_map/while/body/eval_jaxpr/dot_general | solution.py:46
  95.5 2.7 %fusion.132 = f32[8,1024,128]{2,1,0:T(8,128)} fusion(bf16[1024,8,128]{2,1,0:T(8,128)(2,1)S(1)} %get-tuple-element.238, bf16[128,8,192]{2,0,1:T(8,128)(2,1)S(1)} %get-tuple-element.280), kind=kOutput, calls=%fused_computation.7.clone.1 | convolution fusion | flops 268435456 | bytes 6553600 | tf_op jit(solution)/shard_map/while/body/eval_jaxpr/qhd,khd->qhk/dot_general | solution.py:57
  100.6 5.0 %fusion.133 = (f32[128,8]{0,1:T(8,128)S(1)}, f32[128,8,1024]{0,2,1:T(8,128)}) fusion(bf16[128,8,192]{0,2,1:T(8,128)(2,1)S(1)} %copy.109, bf16[1024,32]{0,1:T(8,128)(2,1)} %get-tuple-element.236, bf16[1024,32]{0,1:T(8,128)(2,1)} %get-tuple-element.237, f32[8,1024,128]{2,1,0:T(8,128)} %fusion.132), kind=kOutput, calls=%fused_computation.121.clone.1 | convolution fusion | flops 136576000 | bytes 8654848 | tf_op jit(solution)/shard_map/while/body/eval_jaxpr/qhr,kr->qhk/dot_general | solution.py:63
  105.6 2.9 %fusion.134 = f32[128,8]{0,1:T(8,128)S(1)} fusion(f32[128,8,1024]{0,2,1:T(8,128)} %get-tuple-element.240, f32[128,8]{0,1:T(8,128)S(1)} %select_maximum_fusion.2), kind=kLoop, calls=%fused_computation.4.clone.1 | loop fusion | flops 2096128 | bytes 4202496 | tf_op jit(solution)/shard_map/while/body/eval_jaxpr/reduce_sum | solution.py:72
  112.7 3.9 %all_to_all.29 = bf16[2,64,1024]{2,1,0:T(8,128)(2,1)S(1)} all-to-all(bf16[2,64,1024]{2,1,0:T(8,128)(2,1)S(1)} %all_to_all.20), channel_id=1, replica_groups=mesh['sp'=16,'tp'=2] {'tp'}, dimensions={0} | all-to-all | bytes 524288 | tf_op jit(solution)/shard_map/all_to_all | solution.py:173
  116.7 5.1 %multiply_reduce_fusion = (f32[64]{0:T(128)S(1)}, f32[64,2048]{1,0:T(8,128)S(1)}) fusion(bf16[64,2048]{1,0:T(8,128)(2,1)S(1)} %bitcast.138, bf16[2048,2048]{1,0:T(8,128)(2,1)} %param.28, bf16[64,2048]{1,0:T(8,128)(2,1)S(1)} %copy-done.8), kind=kOutput, calls=%fused_computation.75 | convolution fusion | flops 537657280 | bytes 9437440 | tf_op jit(solution)/shard_map/dot_general | solution.py:174
  121.9 2.1 convolution_convert_fusion.3
  124.1 5.9 %all-to-all-start.1 = ((bf16[16,1,32,2048]{3,2,1,0:T(8,128)(2,1)}), bf16[16,1,32,2048]{3,2,1,0:T(8,128)(2,1)S(1)}, u32[]{:S(2)}, u32[]{:S(2)}) async-start(bf16[16,1,32,2048]{3,2,1,0:T(8,128)(2,1)} %bitcast.4), calls=%async_computation.1 | async-start | bytes 4194304 | tf_op jit(solution)/shard_map/all_to_all | solution.py:201
  131.3 47.0 %all-to-all-done.1 = bf16[16,1,32,2048]{3,2,1,0:T(8,128)(2,1)S(1)} async-done(((bf16[16,1,32,2048]{3,2,1,0:T(8,128)(2,1)}), bf16[16,1,32,2048]{3,2,1,0:T(8,128)(2,1)S(1)}, u32[]{:S(2)}, u32[]{:S(2)}) %all-to-all-start.1) | async-done | bytes 2097184 | tf_op jit(solution)/shard_map/all_to_all | solution.py:201
  178.3 3.8 %fusion.51 = f32[16,1,32,512]{3,2,0,1:T(8,128)} fusion(bf16[1,2048,512]{2,1,0:T(8,128)(2,1)} %all-gather.7.cloned.1.call-done, bf16[16,1,32,2048]{3,2,1,0:T(8,128)(2,1)S(1)} %all-to-all-done.1), kind=kOutput, calls=%fused_computation.65 | convolution fusion | flops 1073741824 | bytes 5242880 | tf_op jit(solution)/shard_map/secd,edf->secf/dot_general | solution.py:202
  182.2 3.2 %fusion.66 = bf16[16,1,32,512]{3,2,0,1:T(8,128)(2,1)S(1)} fusion(bf16[1,2048,512]{2,1,0:T(8,128)(2,1)} %all-gather.9.cloned.1.call-done, bf16[16,1,32,2048]{3,2,1,0:T(8,128)(2,1)S(1)} %all-to-all-done.1, f32[16,1,32,512]{3,2,0,1:T(8,128)} %fusion.51), kind=kOutput, calls=%fused_computation.68 | convolution fusion | flops 1075314688 | bytes 5767168 | tf_op jit(solution)/shard_map/secd,edf->secf/dot_general | solution.py:203
  189.5 5.2 %all-to-all-start.2 = ((bf16[16,1,32,2048]{3,2,1,0:T(8,128)(2,1)}), bf16[16,1,32,2048]{3,2,1,0:T(8,128)(2,1)}, u32[]{:S(2)}, u32[]{:S(2)}) async-start(bf16[16,1,32,2048]{3,2,1,0:T(8,128)(2,1)} %fusion.40), calls=%async_computation.2 | async-start | bytes 4194304 | tf_op jit(solution)/shard_map/all_to_all | solution.py:219
  196.0 46.5 %all-to-all-done.2 = bf16[16,1,32,2048]{3,2,1,0:T(8,128)(2,1)} async-done(((bf16[16,1,32,2048]{3,2,1,0:T(8,128)(2,1)}), bf16[16,1,32,2048]{3,2,1,0:T(8,128)(2,1)}, u32[]{:S(2)}, u32[]{:S(2)}) %all-to-all-start.2) | async-done | bytes 2097184 | tf_op jit(solution)/shard_map/all_to_all | solution.py:219
  242.6 3.1 %convolution_add_fusion.1 = f32[64,2048]{1,0:T(8,128)} fusion(f32[64,2048]{1,0:T(8,128)} %copy-done.5, bf16[64,512]{1,0:T(8,128)(2,1)} %fusion.77, bf16[512,2048]{1,0:T(8,128)(2,1)} %bitcast.28), kind=kOutput, calls=%fused_computation.53 | convolution fusion | flops 134348800 | bytes 3211264 | tf_op jit(solution)/shard_map/dot_general | solution.py:220
  245.7 3.9 %fusion.43 = bf16[64,2048]{1,0:T(8,128)(2,1)} fusion(f32[64,2048]{1,0:T(8,128)} %convolution_add_fusion.1, bf16[512,2048]{1,0:T(8,128)(2,1)} %param.37, bf16[64,2048]{1,0:T(8,128)(2,1)S(1)} %multiply_convert_fusion, bf16[2048,512]{1,0:T(8,128)(2,1)} %param.36, f32[64,512]{1,0:T(8,128)S(1)} %fusion.96), kind=kOutput, calls=%fused_computation.57 | convolution fusion | flops 268894208 | bytes 5373952 | tf_op jit(solution)/shard_map/dot_general | solution.py:229
  (126 shorter events, 32.9 us)
Async XLA Ops:
  6.5 3.5 %copy-start = (bf16[512,3072]{1,0:T(8,128)(2,1)S(1)}, bf16[512,3072]{1,0:T(8,128)(2,1)}, u32[]{:S(2)}) copy-start(bf16[512,3072]{1,0:T(8,128)(2,1)} %param.26) | copy-start | bytes 9437188
  6.5 59.3 %all-gather.5.cloned.1.call-start = ((), (), s32[]{:S(2)}) async-start(), calls=%async_computation.3 | async-start | bytes 1114112 | tf_op jit(solution)/shard_map/all_gather | solution.py:88
  7.3 124.0 %all-gather.7.cloned.1.call-start = ((), (), s32[]{:S(2)}) async-start(), calls=%async_computation.4 | async-start | bytes 3145728 | tf_op jit(solution)/shard_map/all_gather | solution.py:127
  12.3 38.2 %copy-start.15 = (s32[64,4]{0,1:T(4,128)S(1)}, s32[64,4]{0,1:T(4,128)}, u32[]{:S(2)}) copy-start(s32[64,4]{0,1:T(4,128)} %param.30) | copy-start | bytes 3076
  14.0 51.8 %copy-start.10 = (f32[256]{0:T(256)S(1)}, f32[256]{0:T(256)}, u32[]{:S(2)}) copy-start(f32[256]{0:T(256)} %param.25) | copy-start | bytes 3076
  50.5 15.3 %copy-start.11 = (s32[64,4]{0,1:T(4,128)}, s32[64,4]{0,1:T(4,128)S(1)}, u32[]{:S(2)}) copy-start(s32[64,4]{0,1:T(4,128)S(1)} %multiply_add_fusion) | copy-start | bytes 3076
  65.8 5.2 %copy-start.17 = (s32[2]{0:T(128)}, s32[2]{0:T(128)S(1)}, u32[]{:S(2)}) copy-start(s32[2]{0:T(128)S(1)} %get-tuple-element.276) | copy-start | bytes 28 | tf_op jit(solution)/shard_map/while
  77.9 7.9 %copy-start.3 = (f32[128,8,128]{0,2,1:T(8,128)S(1)}, f32[128,8,128]{0,2,1:T(8,128)}, u32[]{:S(2)}) copy-start(f32[128,8,128]{0,2,1:T(8,128)} %get-tuple-element.261) | copy-start | bytes 1572868 | tf_op jit(solution)/shard_map/while
  83.0 3.4 %copy-start.2 = (f32[128,8,1024]{0,2,1:T(8,128)S(1)}, f32[128,8,1024]{0,2,1:T(8,128)}, u32[]{:S(2)}) copy-start(f32[128,8,1024]{0,2,1:T(8,128)} %get-tuple-element.240) | copy-start | bytes 12582916 | tf_op jit(solution)/shard_map/while
  88.6 5.2 %copy-start.17 = (s32[2]{0:T(128)}, s32[2]{0:T(128)S(1)}, u32[]{:S(2)}) copy-start(s32[2]{0:T(128)S(1)} %get-tuple-element.276) | copy-start | bytes 28 | tf_op jit(solution)/shard_map/while
  100.6 7.9 %copy-start.3 = (f32[128,8,128]{0,2,1:T(8,128)S(1)}, f32[128,8,128]{0,2,1:T(8,128)}, u32[]{:S(2)}) copy-start(f32[128,8,128]{0,2,1:T(8,128)} %get-tuple-element.261) | copy-start | bytes 1572868 | tf_op jit(solution)/shard_map/while
  105.6 3.4 %copy-start.2 = (f32[128,8,1024]{0,2,1:T(8,128)S(1)}, f32[128,8,1024]{0,2,1:T(8,128)}, u32[]{:S(2)}) copy-start(f32[128,8,1024]{0,2,1:T(8,128)} %get-tuple-element.240) | copy-start | bytes 12582916 | tf_op jit(solution)/shard_map/while
  111.2 5.4 %copy-start.8 = (bf16[64,2048]{1,0:T(8,128)(2,1)S(1)}, bf16[64,2048]{1,0:T(8,128)(2,1)}, u32[]{:S(2)}) copy-start(bf16[64,2048]{1,0:T(8,128)(2,1)} %param.20) | copy-start | bytes 786436
  116.7 5.1 %copy-start.14 = (f32[2048]{0:T(1024)S(1)}, f32[2048]{0:T(1024)}, u32[]{:S(2)}) copy-start(f32[2048]{0:T(1024)} %param.29) | copy-start | bytes 24580
  116.7 5.2 %copy-start.9 = (pred[64,512]{1,0:T(8,128)(4,1)S(1)}, pred[64,512]{1,0:T(8,128)(4,1)}, u32[]{:S(2)}) copy-start(pred[64,512]{1,0:T(8,128)(4,1)} %fusion.72) | copy-start | bytes 98308
  121.8 2.3 copy-start.5
  124.1 54.3 %all-to-all-start.1 = ((bf16[16,1,32,2048]{3,2,1,0:T(8,128)(2,1)}), bf16[16,1,32,2048]{3,2,1,0:T(8,128)(2,1)S(1)}, u32[]{:S(2)}, u32[]{:S(2)}) async-start(bf16[16,1,32,2048]{3,2,1,0:T(8,128)(2,1)} %bitcast.4), calls=%async_computation.1 | async-start | bytes 4194304 | tf_op jit(solution)/shard_map/all_to_all | solution.py:201
  130.0 52.2 %all-gather.9.cloned.1.call-start = ((), (), s32[]{:S(2)}) async-start(), calls=%async_computation.5 | async-start | bytes 3145728 | tf_op jit(solution)/shard_map/all_gather | solution.py:128
  130.7 54.7 %all-gather.11.cloned.1.call-start = ((), (), s32[]{:S(2)}) async-start(), calls=%async_computation.6 | async-start | bytes 3145728 | tf_op jit(solution)/shard_map/all_gather | solution.py:129
  189.5 5.2 %copy-start.16 = (f32[64,4]{0,1:T(4,128)S(1)}, f32[64,4]{0,1:T(4,128)}, u32[]{:S(2)}) copy-start(f32[64,4]{0,1:T(4,128)} %param.31) | copy-start | bytes 3076
  189.5 5.2 %copy-start.12 = (s32[64,4]{0,1:T(4,128)S(1)}, s32[64,4]{0,1:T(4,128)}, u32[]{:S(2)}) copy-start(s32[64,4]{0,1:T(4,128)} %copy-done.11) | copy-start | bytes 3076
  189.5 6.0 %copy-start.6 = (bf16[2048,512]{1,0:T(8,128)(2,1)S(1)}, bf16[2048,512]{1,0:T(8,128)(2,1)}, u32[]{:S(2)}) copy-start(bf16[2048,512]{1,0:T(8,128)(2,1)} %param.35) | copy-start | bytes 6291460
  189.5 53.0 %all-to-all-start.2 = ((bf16[16,1,32,2048]{3,2,1,0:T(8,128)(2,1)}), bf16[16,1,32,2048]{3,2,1,0:T(8,128)(2,1)}, u32[]{:S(2)}, u32[]{:S(2)}) async-start(bf16[16,1,32,2048]{3,2,1,0:T(8,128)(2,1)} %fusion.40), calls=%async_computation.2 | async-start | bytes 4194304 | tf_op jit(solution)/shard_map/all_to_all | solution.py:219
  242.6 7.1 %copy-start.1 = (bf16[512,3072]{1,0:T(8,128)(2,1)S(1)}, bf16[512,3072]{1,0:T(8,128)(2,1)}, u32[]{:S(2)}) copy-start(bf16[512,3072]{1,0:T(8,128)(2,1)} %param.26) | copy-start | bytes 9437188
  (6 other events, 10.0 us)
Sparse Core Ops, SparseCore 0:
  10.1 55.6 all-gather.4
  67.4 10.2 all-gather.6
  132.3 11.2 all-gather.8
  145.0 11.7 all-gather.10
where the time goes:
time: 257 us; the launch traced here: 256 us
  waiting for transfers between devices  108 us (42%)
  matrix products  51.4 us (20%)
  blocking collectives  39.1 us (15%)
  other arithmetic  17.4 us (7%)
  local copies, waits for them, and re-layouts  13.6 us (5%)
  between operations  13.4 us (5%)
  starting transfers between devices  11.2 us (4%)
    all_to_all x1, waiting for transfers between devices, shards(): lax.all_to_all(outgoing, 'sp', split_axis=0, concat_axis=0, tiled=True)  47 us
    all_to_all x1, waiting for transfers between devices, shards(): lax.all_to_all(summed, 'sp', split_axis=0, concat_axis=0, tiled=True)  46.5 us
    all_gather x1, blocking collectives, attend_all(): rot_piece = lax.all_gather(rot_shard, 'sp', axis=0, tiled=True)  35.2 us
    all_gather x1, waiting for transfers between devices, attend_all(): lat_piece = lax.all_gather(lat_shard, 'sp', axis=0, tiled=True)  12.2 us
    dot_general x2, matrix products, absorb(): jnp.einsum('qhr,kr->qhk', queries[:, :, KEY_PLAIN_WIDTH:], shared_rot, pr...  10 us
    while x26, local copies, waits for them, and re-layouts  6.17 us
    all_to_all x1, starting transfers between devices, shards(): lax.all_to_all(outgoing, 'sp', split_axis=0, concat_axis=0, tiled=True)  5.91 us
    reduce_sum x2, other arithmetic, absorb(): new_sum = run_sum * factor + jnp.sum(weights, axis=-1)  5.81 us
  transfers between devices with their start and end apart: 6, of which 3 were waited for; matrix products, arithmetic and copies ran while one was open for 27% of the time, Pallas kernels for 0%

commit v1 on v0

--- a/solution.py
+++ b/solution.py
@@ -86,7 +86,30 @@
         jnp.zeros((query_rows, head_count, VALUE_HEAD_WIDTH), jnp.float32),
     )
     lat_piece = lax.all_gather(lat_shard, "sp", axis=0, tiled=True)
-    rot_piece = lax.all_gather(rot_shard, "sp", axis=0, tiled=True)
+    later, base_arr, arr_out = (lax.axis_size("sp"), lax.axis_index("sp"), rot_shard.shape[0])
+    items = tuple((k * later if to_i == 0 else k for to_i, k in enumerate(rot_shard.shape)))
+    rot_piece = lax.dynamic_update_slice_in_dim(
+        jnp.zeros(items, rot_shard.dtype), rot_shard, base_arr * arr_out, axis=0
+    )
+    opened = y_new = rot_shard
+    for k0 in [*range(1, later // 2 + 1)]:
+        opened = lax.ppermute(
+            opened,
+            axis_name="sp",
+            perm=tuple(((to_i, (to_i + 1) % later) for to_i in range(later))),
+        )
+        rot_piece = lax.dynamic_update_slice_in_dim(
+            rot_piece, opened, (base_arr - k0) % later * arr_out, axis=0
+        )
+        if 2 * k0 < later:
+            y_new = lax.ppermute(
+                y_new,
+                axis_name="sp",
+                perm=tuple(((to_i, (to_i - 1) % later) for to_i in range(later))),
+            )
+            rot_piece = lax.dynamic_update_slice_in_dim(
+                rot_piece, y_new, (base_arr + k0) % later * arr_out, axis=0
+            )
     span_rows = key_span(lat_piece.shape[0])
     block_total = lat_piece.shape[0] // span_rows
 

time: 257 us -> 267 us (1.039)
  starting transfers between devices: 11.2 us -> 46.8 us
  blocking collectives: 39.1 us -> 3.94 us
  local copies, waits for them, and re-layouts: 13.6 us -> 24.2 us
    all_gather x1 -> x0, blocking collectives: 35.2 us -> none  [attend_all(): rot_piece = lax.all_gather(rot_shard, 'sp', axis=0, tiled=True)]
    ppermute x0 -> x15, starting transfers between devices: none -> 26.3 us  [the longest x8 19.7 us: attend_all(): lax.ppermute(opened, axis_name='sp', perm=tuple(((to_i, (to_i + 1) % late...]
    dynamic_update_slice x0 -> x16, local copies, waits for them, and re-layouts: none -> 9.7 us  [the longest x8 4.85 us: attend_all(): lax.dynamic_update_slice_in_dim(rot_piece, opened, (base_arr - k0) % late...]
    all_to_all x1, starting transfers between devices: 5.91 us -> 14.8 us  [shards(): lax.all_to_all(outgoing, 'sp', split_axis=0, concat_axis=0, tiled=True)]
    all_gather x1, waiting for transfers between devices: 12.2 us -> 7.93 us  [attend_all(): lat_piece = lax.all_gather(lat_shard, 'sp', axis=0, tiled=True)]
    ppermute x0 -> x15, waiting for transfers between devices: none -> 3.64 us  [the longest x7 1.98 us: attend_all(): lax.ppermute(y_new, axis_name='sp', perm=tuple(((to_i, (to_i - 1) % later...]
  transfers between devices with their start and end apart: 6 -> 21, of which waited for: 3 -> 12; matrix products, arithmetic and copies ran while one was open for 27% -> 30% of each run, Pallas kernels for 0% -> 0%
where the time goes in v1:
time: 267 us; the launch traced here: 266 us
  waiting for transfers between devices  107 us (40%)
  matrix products  51.3 us (19%)
  starting transfers between devices  46.8 us (18%)
  local copies, waits for them, and re-layouts  24.2 us (9%)
  other arithmetic  17.5 us (7%)
  between operations  13.5 us (5%)
  blocking collectives  3.94 us (1%)
    all_to_all x1, waiting for transfers between devices, shards(): lax.all_to_all(outgoing, 'sp', split_axis=0, concat_axis=0, tiled=True)  47.2 us
    all_to_all x1, waiting for transfers between devices, shards(): lax.all_to_all(summed, 'sp', split_axis=0, concat_axis=0, tiled=True)  46.7 us
    ppermute x8, starting transfers between devices, attend_all(): lax.ppermute(opened, axis_name='sp', perm=tuple(((to_i, (to_i + 1) % late...  19.7 us
    all_to_all x1, starting transfers between devices, shards(): lax.all_to_all(outgoing, 'sp', split_axis=0, concat_axis=0, tiled=True)  14.8 us
    dot_general x2, matrix products, absorb(): jnp.einsum('qhr,kr->qhk', queries[:, :, KEY_PLAIN_WIDTH:], shared_rot, pr...  9.99 us
    all_gather x1, waiting for transfers between devices, attend_all(): lat_piece = lax.all_gather(lat_shard, 'sp', axis=0, tiled=True)  7.93 us
    ppermute x7, starting transfers between devices, attend_all(): lax.ppermute(y_new, axis_name='sp', perm=tuple(((to_i, (to_i - 1) % later...  6.58 us
    while x26, local copies, waits for them, and re-layouts  6.21 us
  transfers between devices with their start and end apart: 21, of which 12 were waited for; matrix products, arithmetic and copies ran while one was open for 30% of the time, Pallas kernels for 0%

profile of v1, /device:TPU:12, one launch (start us, length us, event | category | flops | bytes accessed | tf_op | source)
XLA Modules:
  0.0 266.2 jit_solution(5440240893028061653)
XLA Ops:
  36.2 2.8 %collective-permute-start.8 = (bf16[128,64]{0,1:T(8,128)(2,1)S(1)}, bf16[128,64]{0,1:T(8,128)(2,1)S(1)}, u32[]{:S(2)}, u32[]{:S(2)}) collective-permute-start(bf16[128,64]{0,1:T(8,128)(2,1)S(1)} %collective-permute-done.6), channel_id=1, source_target_pairs={{0,2},{2,4},{4,6},{6,8},{8,10},{10,12},{12,14},{14,16},{16,18},{18... | collective-permute-start | bytes 49160 | tf_op jit(solution)/shard_map/ppermute | solution.py:96
  41.0 3.7 %collective-permute-start.10 = (bf16[128,64]{0,1:T(8,128)(2,1)S(1)}, bf16[128,64]{0,1:T(8,128)(2,1)S(1)}, u32[]{:S(2)}, u32[]{:S(2)}) collective-permute-start(bf16[128,64]{0,1:T(8,128)(2,1)S(1)} %collective-permute-done.8), channel_id=1, source_target_pairs={{0,2},{2,4},{4,6},{6,8},{8,10},{10,12},{12,14},{14,16},{16,18},{18... | collective-permute-start | bytes 49160 | tf_op jit(solution)/shard_map/ppermute | solution.py:96
  46.2 4.2 %collective-permute-start.12 = (bf16[128,64]{0,1:T(8,128)(2,1)S(1)}, bf16[128,64]{0,1:T(8,128)(2,1)S(1)}, u32[]{:S(2)}, u32[]{:S(2)}) collective-permute-start(bf16[128,64]{0,1:T(8,128)(2,1)S(1)} %collective-permute-done.10), channel_id=1, source_target_pairs={{0,2},{2,4},{4,6},{6,8},{8,10},{10,12},{12,14},{14,16},{16,18},{18... | collective-permute-start | bytes 49160 | tf_op jit(solution)/shard_map/ppermute | solution.py:96
  51.9 4.4 %collective-permute-start.14 = (bf16[128,64]{0,1:T(8,128)(2,1)S(1)}, bf16[128,64]{0,1:T(8,128)(2,1)S(1)}, u32[]{:S(2)}, u32[]{:S(2)}) collective-permute-start(bf16[128,64]{0,1:T(8,128)(2,1)S(1)} %collective-permute-done.12), channel_id=1, source_target_pairs={{0,2},{2,4},{4,6},{6,8},{8,10},{10,12},{12,14},{14,16},{16,18},{18... | collective-permute-start | bytes 49160 | tf_op jit(solution)/shard_map/ppermute | solution.py:96
  58.3 7.9 %all-gather.5.cloned.1.call-done = bf16[2048,256]{1,0:T(8,128)(2,1)} async-done(((bf16[128,256]{1,0:T(8,128)(2,1)}), bf16[2048,256]{1,0:T(8,128)(2,1)}) %all-gather.5.cloned.1.call-update) | async-done | bytes 1048592 | tf_op jit(solution)/shard_map/all_gather | solution.py:88
  66.3 45.4 %while.15 = (s32[]{:T(128)}, f32[128,8]{0,1:T(8,128)S(1)}, f32[128,8]{0,1:T(8,128)S(1)}, f32[128,8,128]{0,2,1:T(8,128)}, s32[2]{0:T(128)S(1)}, /*index=5*/bf16[2...) while((s32[]{:T(128)}, f32[128,8]{0,1:T(8,128)S(1)}, ...), condition=%wide.region_5.6_spmd.clone, body=%wide.region_1.5_spmd.clone.sunk | while | flops 1756078208 | bytes 72443560 | solution.py:125
  68.8 2.7 %convolution_convert_fusion.5 = bf16[1024,2048]{1,0:T(8,128)(2,1)S(1)} fusion(bf16[256,2048]{1,0:T(8,128)(2,1)} %get-tuple-element.279, f32[256]{0:T(256)S(1)} %get-tuple-element.278, f32[1024]{0:T(1024)S(1)} %add_rsqrt_fusion.4, bf16[2048,256]{1,0:T(8,128)(2,1)} %get-tuple-element.277, s32[]{:T(128)S(6)} %select_n.164), kind=kOutput, calls=%fused_computation.2.clone.1 | convolution fusion | flops 1076887552 | bytes 5772292 | tf_op jit(solution)/shard_map/while/body/eval_jaxpr/dot_general | solution.py:46
  73.3 2.7 fusion.132
  78.4 5.0 %fusion.133 = (f32[128,8]{0,1:T(8,128)S(1)}, f32[128,8,1024]{0,2,1:T(8,128)}) fusion(bf16[128,8,192]{0,2,1:T(8,128)(2,1)S(1)} %copy.109, bf16[1024,32]{0,1:T(8,128)(2,1)} %get-tuple-element.236, bf16[1024,32]{0,1:T(8,128)(2,1)} %get-tuple-element.237, f32[8,1024,128]{2,1,0:T(8,128)} %fusion.132), kind=kOutput, calls=%fused_computation.137.clone.1 | convolution fusion | flops 136576000 | bytes 8654848 | tf_op jit(solution)/shard_map/while/body/eval_jaxpr/qhr,kr->qhk/dot_general | solution.py:63
  83.4 2.9 %fusion.134 = f32[128,8]{0,1:T(8,128)S(1)} fusion(f32[128,8,1024]{0,2,1:T(8,128)} %get-tuple-element.240, f32[128,8]{0,1:T(8,128)S(1)} %select_maximum_fusion.2), kind=kLoop, calls=%fused_computation.4.clone.1 | loop fusion | flops 2096128 | bytes 4202496 | tf_op jit(solution)/shard_map/while/body/eval_jaxpr/reduce_sum | solution.py:72
  91.5 2.7 %convolution_convert_fusion.5 = bf16[1024,2048]{1,0:T(8,128)(2,1)S(1)} fusion(bf16[256,2048]{1,0:T(8,128)(2,1)} %get-tuple-element.279, f32[256]{0:T(256)S(1)} %get-tuple-element.278, f32[1024]{0:T(1024)S(1)} %add_rsqrt_fusion.4, bf16[2048,256]{1,0:T(8,128)(2,1)} %get-tuple-element.277, s32[]{:T(128)S(6)} %select_n.164), kind=kOutput, calls=%fused_computation.2.clone.1 | convolution fusion | flops 1076887552 | bytes 5772292 | tf_op jit(solution)/shard_map/while/body/eval_jaxpr/dot_general | solution.py:46
  96.0 2.7 fusion.132
  101.1 5.0 %fusion.133 = (f32[128,8]{0,1:T(8,128)S(1)}, f32[128,8,1024]{0,2,1:T(8,128)}) fusion(bf16[128,8,192]{0,2,1:T(8,128)(2,1)S(1)} %copy.109, bf16[1024,32]{0,1:T(8,128)(2,1)} %get-tuple-element.236, bf16[1024,32]{0,1:T(8,128)(2,1)} %get-tuple-element.237, f32[8,1024,128]{2,1,0:T(8,128)} %fusion.132), kind=kOutput, calls=%fused_computation.137.clone.1 | convolution fusion | flops 136576000 | bytes 8654848 | tf_op jit(solution)/shard_map/while/body/eval_jaxpr/qhr,kr->qhk/dot_general | solution.py:63
  106.1 2.9 %fusion.134 = f32[128,8]{0,1:T(8,128)S(1)} fusion(f32[128,8,1024]{0,2,1:T(8,128)} %get-tuple-element.240, f32[128,8]{0,1:T(8,128)S(1)} %select_maximum_fusion.2), kind=kLoop, calls=%fused_computation.4.clone.1 | loop fusion | flops 2096128 | bytes 4202496 | tf_op jit(solution)/shard_map/while/body/eval_jaxpr/reduce_sum | solution.py:72
  113.2 3.9 %all_to_all.29 = bf16[2,64,1024]{2,1,0:T(8,128)(2,1)S(1)} all-to-all(bf16[2,64,1024]{2,1,0:T(8,128)(2,1)S(1)} %all_to_all.20), channel_id=1, replica_groups=mesh['sp'=16,'tp'=2] {'tp'}, dimensions={0} | all-to-all | bytes 524288 | tf_op jit(solution)/shard_map/all_to_all | solution.py:196
  117.2 5.1 %multiply_reduce_fusion = (f32[64]{0:T(128)S(1)}, f32[64,2048]{1,0:T(8,128)S(1)}) fusion(bf16[64,2048]{1,0:T(8,128)(2,1)S(1)} %bitcast.138, bf16[2048,2048]{1,0:T(8,128)(2,1)} %param.28, bf16[64,2048]{1,0:T(8,128)(2,1)S(1)} %copy-done.8), kind=kOutput, calls=%fused_computation.75 | convolution fusion | flops 537657280 | bytes 9437440 | tf_op jit(solution)/shard_map/dot_general | solution.py:197
  124.5 14.8 %all-to-all-start.1 = ((bf16[16,1,32,2048]{3,2,1,0:T(8,128)(2,1)}), bf16[16,1,32,2048]{3,2,1,0:T(8,128)(2,1)S(1)}, u32[]{:S(2)}, u32[]{:S(2)}) async-start(bf16[16,1,32,2048]{3,2,1,0:T(8,128)(2,1)} %bitcast.4), calls=%async_computation.1 | async-start | bytes 4194304 | tf_op jit(solution)/shard_map/all_to_all | solution.py:224
  140.7 47.2 %all-to-all-done.1 = bf16[16,1,32,2048]{3,2,1,0:T(8,128)(2,1)S(1)} async-done(((bf16[16,1,32,2048]{3,2,1,0:T(8,128)(2,1)}), bf16[16,1,32,2048]{3,2,1,0:T(8,128)(2,1)S(1)}, u32[]{:S(2)}, u32[]{:S(2)}) %all-to-all-start.1) | async-done | bytes 2097184 | tf_op jit(solution)/shard_map/all_to_all | solution.py:224
  187.9 3.8 %fusion.51 = f32[16,1,32,512]{3,2,0,1:T(8,128)} fusion(bf16[1,2048,512]{2,1,0:T(8,128)(2,1)} %all-gather.7.cloned.1.call-done, bf16[16,1,32,2048]{3,2,1,0:T(8,128)(2,1)S(1)} %all-to-all-done.1), kind=kOutput, calls=%fused_computation.65 | convolution fusion | flops 1073741824 | bytes 5242880 | tf_op jit(solution)/shard_map/secd,edf->secf/dot_general | solution.py:225
  191.7 3.2 %fusion.66 = bf16[16,1,32,512]{3,2,0,1:T(8,128)(2,1)S(1)} fusion(bf16[1,2048,512]{2,1,0:T(8,128)(2,1)} %all-gather.9.cloned.1.call-done, bf16[16,1,32,2048]{3,2,1,0:T(8,128)(2,1)S(1)} %all-to-all-done.1, f32[16,1,32,512]{3,2,0,1:T(8,128)} %fusion.51), kind=kOutput, calls=%fused_computation.68 | convolution fusion | flops 1075314688 | bytes 5767168 | tf_op jit(solution)/shard_map/secd,edf->secf/dot_general | solution.py:226
  199.1 5.6 %all-to-all-start.2 = ((bf16[16,1,32,2048]{3,2,1,0:T(8,128)(2,1)}), bf16[16,1,32,2048]{3,2,1,0:T(8,128)(2,1)}, u32[]{:S(2)}, u32[]{:S(2)}) async-start(bf16[16,1,32,2048]{3,2,1,0:T(8,128)(2,1)} %fusion.40), calls=%async_computation.2 | async-start | bytes 4194304 | tf_op jit(solution)/shard_map/all_to_all | solution.py:242
  206.0 46.7 %all-to-all-done.2 = bf16[16,1,32,2048]{3,2,1,0:T(8,128)(2,1)} async-done(((bf16[16,1,32,2048]{3,2,1,0:T(8,128)(2,1)}), bf16[16,1,32,2048]{3,2,1,0:T(8,128)(2,1)}, u32[]{:S(2)}, u32[]{:S(2)}) %all-to-all-start.2) | async-done | bytes 2097184 | tf_op jit(solution)/shard_map/all_to_all | solution.py:242
  252.7 3.1 %convolution_add_fusion.1 = f32[64,2048]{1,0:T(8,128)} fusion(f32[64,2048]{1,0:T(8,128)} %copy-done.5, bf16[64,512]{1,0:T(8,128)(2,1)} %fusion.77, bf16[512,2048]{1,0:T(8,128)(2,1)} %bitcast.28), kind=kOutput, calls=%fused_computation.53 | convolution fusion | flops 134348800 | bytes 3211264 | tf_op jit(solution)/shard_map/dot_general | solution.py:243
  255.8 3.9 %fusion.43 = bf16[64,2048]{1,0:T(8,128)(2,1)} fusion(f32[64,2048]{1,0:T(8,128)} %convolution_add_fusion.1, bf16[512,2048]{1,0:T(8,128)(2,1)} %param.37, bf16[64,2048]{1,0:T(8,128)(2,1)S(1)} %multiply_convert_fusion, bf16[2048,512]{1,0:T(8,128)(2,1)} %param.36, f32[64,512]{1,0:T(8,128)S(1)} %fusion.96), kind=kOutput, calls=%fused_computation.57 | convolution fusion | flops 268894208 | bytes 5373952 | tf_op jit(solution)/shard_map/dot_general | solution.py:252
  (172 shorter events, 64.4 us)
Async XLA Ops:
  6.5 59.7 %all-gather.5.cloned.1.call-start = ((), (), s32[]{:S(2)}) async-start(), calls=%async_computation.3 | async-start | bytes 1114112 | tf_op jit(solution)/shard_map/all_gather | solution.py:88
  7.3 133.4 %all-gather.7.cloned.1.call-start = ((), (), s32[]{:S(2)}) async-start(), calls=%async_computation.4 | async-start | bytes 3145728 | tf_op jit(solution)/shard_map/all_gather | solution.py:150
  7.3 14.9 %collective-permute-start = (bf16[128,64]{0,1:T(8,128)(2,1)}, bf16[128,64]{0,1:T(8,128)(2,1)S(1)}, u32[]{:S(2)}, u32[]{:S(2)}) collective-permute-start(bf16[128,64]{0,1:T(8,128)(2,1)} %param.23), channel_id=1, source_target_pairs={{0,2},{2,4},{4,6},{6,8},{8,10},{10,12},{12,14},{14,16},{16,18},{18... | collective-permute-start | bytes 49160 | tf_op jit(solution)/shard_map/ppermute | solution.py:96
  8.8 14.0 %collective-permute-start.1 = (bf16[128,64]{0,1:T(8,128)(2,1)}, bf16[128,64]{0,1:T(8,128)(2,1)S(1)}, u32[]{:S(2)}, u32[]{:S(2)}) collective-permute-start(bf16[128,64]{0,1:T(8,128)(2,1)} %param.23), channel_id=1, source_target_pairs={{0,30},{2,0},{4,2},{6,4},{8,6},{10,8},{12,10},{14,12},{16,14},{18,... | collective-permute-start | bytes 49160 | tf_op jit(solution)/shard_map/ppermute | solution.py:105
  18.2 48.1 %copy-start.10 = (f32[256]{0:T(256)S(1)}, f32[256]{0:T(256)}, u32[]{:S(2)}) copy-start(f32[256]{0:T(256)} %param.25) | copy-start | bytes 3076
  22.3 4.7 %collective-permute-start.2 = (bf16[128,64]{0,1:T(8,128)(2,1)S(1)}, bf16[128,64]{0,1:T(8,128)(2,1)S(1)}, u32[]{:S(2)}, u32[]{:S(2)}) collective-permute-start(bf16[128,64]{0,1:T(8,128)(2,1)S(1)} %collective-permute-done), channel_id=1, source_target_pairs={{0,2},{2,4},{4,6},{6,8},{8,10},{10,12},{12,14},{14,16},{16,18},{18... | collective-permute-start | bytes 49160 | tf_op jit(solution)/shard_map/ppermute | solution.py:96
  22.9 5.1 %collective-permute-start.3 = (bf16[128,64]{0,1:T(8,128)(2,1)S(1)}, bf16[128,64]{0,1:T(8,128)(2,1)S(1)}, u32[]{:S(2)}, u32[]{:S(2)}) collective-permute-start(bf16[128,64]{0,1:T(8,128)(2,1)S(1)} %collective-permute-done.1), channel_id=1, source_target_pairs={{0,30},{2,0},{4,2},{6,4},{8,6},{10,8},{12,10},{14,12},{16,14},{18,... | collective-permute-start | bytes 49160 | tf_op jit(solution)/shard_map/ppermute | solution.py:105
  26.9 4.6 %collective-permute-start.4 = (bf16[128,64]{0,1:T(8,128)(2,1)S(1)}, bf16[128,64]{0,1:T(8,128)(2,1)S(1)}, u32[]{:S(2)}, u32[]{:S(2)}) collective-permute-start(bf16[128,64]{0,1:T(8,128)(2,1)S(1)} %collective-permute-done.2), channel_id=1, source_target_pairs={{0,2},{2,4},{4,6},{6,8},{8,10},{10,12},{12,14},{14,16},{16,18},{18... | collective-permute-start | bytes 49160 | tf_op jit(solution)/shard_map/ppermute | solution.py:96
  28.0 5.7 %collective-permute-start.5 = (bf16[128,64]{0,1:T(8,128)(2,1)S(1)}, bf16[128,64]{0,1:T(8,128)(2,1)S(1)}, u32[]{:S(2)}, u32[]{:S(2)}) collective-permute-start(bf16[128,64]{0,1:T(8,128)(2,1)S(1)} %collective-permute-done.3), channel_id=1, source_target_pairs={{0,30},{2,0},{4,2},{6,4},{8,6},{10,8},{12,10},{14,12},{16,14},{18,... | collective-permute-start | bytes 49160 | tf_op jit(solution)/shard_map/ppermute | solution.py:105
  31.6 4.6 %collective-permute-start.6 = (bf16[128,64]{0,1:T(8,128)(2,1)S(1)}, bf16[128,64]{0,1:T(8,128)(2,1)S(1)}, u32[]{:S(2)}, u32[]{:S(2)}) collective-permute-start(bf16[128,64]{0,1:T(8,128)(2,1)S(1)} %collective-permute-done.4), channel_id=1, source_target_pairs={{0,2},{2,4},{4,6},{6,8},{8,10},{10,12},{12,14},{14,16},{16,18},{18... | collective-permute-start | bytes 49160 | tf_op jit(solution)/shard_map/ppermute | solution.py:96
  33.7 6.1 %collective-permute-start.7 = (bf16[128,64]{0,1:T(8,128)(2,1)S(1)}, bf16[128,64]{0,1:T(8,128)(2,1)S(1)}, u32[]{:S(2)}, u32[]{:S(2)}) collective-permute-start(bf16[128,64]{0,1:T(8,128)(2,1)S(1)} %collective-permute-done.5), channel_id=1, source_target_pairs={{0,30},{2,0},{4,2},{6,4},{8,6},{10,8},{12,10},{14,12},{16,14},{18,... | collective-permute-start | bytes 49160 | tf_op jit(solution)/shard_map/ppermute | solution.py:105
  36.2 4.7 %collective-permute-start.8 = (bf16[128,64]{0,1:T(8,128)(2,1)S(1)}, bf16[128,64]{0,1:T(8,128)(2,1)S(1)}, u32[]{:S(2)}, u32[]{:S(2)}) collective-permute-start(bf16[128,64]{0,1:T(8,128)(2,1)S(1)} %collective-permute-done.6), channel_id=1, source_target_pairs={{0,2},{2,4},{4,6},{6,8},{8,10},{10,12},{12,14},{14,16},{16,18},{18... | collective-permute-start | bytes 49160 | tf_op jit(solution)/shard_map/ppermute | solution.py:96
  39.7 5.2 %collective-permute-start.9 = (bf16[128,64]{0,1:T(8,128)(2,1)S(1)}, bf16[128,64]{0,1:T(8,128)(2,1)S(1)}, u32[]{:S(2)}, u32[]{:S(2)}) collective-permute-start(bf16[128,64]{0,1:T(8,128)(2,1)S(1)} %collective-permute-done.7), channel_id=1, source_target_pairs={{0,30},{2,0},{4,2},{6,4},{8,6},{10,8},{12,10},{14,12},{16,14},{18,... | collective-permute-start | bytes 49160 | tf_op jit(solution)/shard_map/ppermute | solution.py:105
  41.0 5.2 %collective-permute-start.10 = (bf16[128,64]{0,1:T(8,128)(2,1)S(1)}, bf16[128,64]{0,1:T(8,128)(2,1)S(1)}, u32[]{:S(2)}, u32[]{:S(2)}) collective-permute-start(bf16[128,64]{0,1:T(8,128)(2,1)S(1)} %collective-permute-done.8), channel_id=1, source_target_pairs={{0,2},{2,4},{4,6},{6,8},{8,10},{10,12},{12,14},{14,16},{16,18},{18... | collective-permute-start | bytes 49160 | tf_op jit(solution)/shard_map/ppermute | solution.py:96
  45.0 5.7 %collective-permute-start.11 = (bf16[128,64]{0,1:T(8,128)(2,1)S(1)}, bf16[128,64]{0,1:T(8,128)(2,1)S(1)}, u32[]{:S(2)}, u32[]{:S(2)}) collective-permute-start(bf16[128,64]{0,1:T(8,128)(2,1)S(1)} %collective-permute-done.9), channel_id=1, source_target_pairs={{0,30},{2,0},{4,2},{6,4},{8,6},{10,8},{12,10},{14,12},{16,14},{18,... | collective-permute-start | bytes 49160 | tf_op jit(solution)/shard_map/ppermute | solution.py:105
  46.2 5.7 %collective-permute-start.12 = (bf16[128,64]{0,1:T(8,128)(2,1)S(1)}, bf16[128,64]{0,1:T(8,128)(2,1)S(1)}, u32[]{:S(2)}, u32[]{:S(2)}) collective-permute-start(bf16[128,64]{0,1:T(8,128)(2,1)S(1)} %collective-permute-done.10), channel_id=1, source_target_pairs={{0,2},{2,4},{4,6},{6,8},{8,10},{10,12},{12,14},{14,16},{16,18},{18... | collective-permute-start | bytes 49160 | tf_op jit(solution)/shard_map/ppermute | solution.py:96
  50.7 6.2 %collective-permute-start.13 = (bf16[128,64]{0,1:T(8,128)(2,1)S(1)}, bf16[128,64]{0,1:T(8,128)(2,1)S(1)}, u32[]{:S(2)}, u32[]{:S(2)}) collective-permute-start(bf16[128,64]{0,1:T(8,128)(2,1)S(1)} %collective-permute-done.11), channel_id=1, source_target_pairs={{0,30},{2,0},{4,2},{6,4},{8,6},{10,8},{12,10},{14,12},{16,14},{18,... | collective-permute-start | bytes 49160 | tf_op jit(solution)/shard_map/ppermute | solution.py:105
  51.9 5.9 %collective-permute-start.14 = (bf16[128,64]{0,1:T(8,128)(2,1)S(1)}, bf16[128,64]{0,1:T(8,128)(2,1)S(1)}, u32[]{:S(2)}, u32[]{:S(2)}) collective-permute-start(bf16[128,64]{0,1:T(8,128)(2,1)S(1)} %collective-permute-done.12), channel_id=1, source_target_pairs={{0,2},{2,4},{4,6},{6,8},{8,10},{10,12},{12,14},{14,16},{16,18},{18... | collective-permute-start | bytes 49160 | tf_op jit(solution)/shard_map/ppermute | solution.py:96
  78.4 7.9 %copy-start.3 = (f32[128,8,128]{0,2,1:T(8,128)S(1)}, f32[128,8,128]{0,2,1:T(8,128)}, u32[]{:S(2)}) copy-start(f32[128,8,128]{0,2,1:T(8,128)} %get-tuple-element.261) | copy-start | bytes 1572868 | tf_op jit(solution)/shard_map/while
  101.1 7.9 %copy-start.3 = (f32[128,8,128]{0,2,1:T(8,128)S(1)}, f32[128,8,128]{0,2,1:T(8,128)}, u32[]{:S(2)}) copy-start(f32[128,8,128]{0,2,1:T(8,128)} %get-tuple-element.261) | copy-start | bytes 1572868 | tf_op jit(solution)/shard_map/while
  124.5 63.4 %all-to-all-start.1 = ((bf16[16,1,32,2048]{3,2,1,0:T(8,128)(2,1)}), bf16[16,1,32,2048]{3,2,1,0:T(8,128)(2,1)S(1)}, u32[]{:S(2)}, u32[]{:S(2)}) async-start(bf16[16,1,32,2048]{3,2,1,0:T(8,128)(2,1)} %bitcast.4), calls=%async_computation.1 | async-start | bytes 4194304 | tf_op jit(solution)/shard_map/all_to_all | solution.py:224
  139.3 52.4 %all-gather.9.cloned.1.call-start = ((), (), s32[]{:S(2)}) async-start(), calls=%async_computation.5 | async-start | bytes 3145728 | tf_op jit(solution)/shard_map/all_gather | solution.py:151
  140.1 54.9 %all-gather.11.cloned.1.call-start = ((), (), s32[]{:S(2)}) async-start(), calls=%async_computation.6 | async-start | bytes 3145728 | tf_op jit(solution)/shard_map/all_gather | solution.py:152
  199.1 53.6 %all-to-all-start.2 = ((bf16[16,1,32,2048]{3,2,1,0:T(8,128)(2,1)}), bf16[16,1,32,2048]{3,2,1,0:T(8,128)(2,1)}, u32[]{:S(2)}, u32[]{:S(2)}) async-start(bf16[16,1,32,2048]{3,2,1,0:T(8,128)(2,1)} %fusion.40), calls=%async_computation.2 | async-start | bytes 4194304 | tf_op jit(solution)/shard_map/all_to_all | solution.py:242
  (21 other events, 85.0 us)
Sparse Core Ops, SparseCore 0:
  10.1 56.1 all-gather.4
  67.8 10.0 all-gather.6
  141.7 11.3 all-gather.8
  154.4 11.7 all-gather.10
